TPU v7x, 32 devices: a whole 2x2x4 slice. The times are simulated.
32 devices in a mesh: sp: 8 (over z, x), tp: 4 (over y, core).
Axes of the slice: x: 2, y: 2, z: 4, core: 2. Of those that a mesh axis runs over, the one named last changes fastest.
Arguments:
- features: bfloat16 [3072, 2048], P('sp', 'tp'), may hold values from -6 to 6
- norm_gain: float32 [2048], replicated, may hold values from 0.28 to 10
- w_query: bfloat16 [2048, 1024], P(None, 'tp'), may hold values from -0.125 to 0.125
- w_key: bfloat16 [2048, 512], P(None, 'tp'), may hold values from -0.125 to 0.125
- w_value: bfloat16 [2048, 512], P(None, 'tp'), may hold values from -0.125 to 0.125
- head_sinks: float32 [16], P('tp'), may hold values from 1 to 5
- w_query_latent: bfloat16 [2048, 512], replicated, may hold values from -0.125 to 0.125
- w_kv_latent: bfloat16 [2048, 512], replicated, may hold values from -0.125 to 0.125
- w_rope_key: bfloat16 [2048, 64], replicated, may hold values from -0.125 to 0.125
- query_latent_gain: float32 [512], replicated, may hold values from 0.28 to 10
- kv_latent_gain: float32 [512], replicated, may hold values from 0.28 to 10
- w_query_content: bfloat16 [512, 1024], P(None, 'tp'), may hold values from -0.25 to 0.25
- w_query_rotary: bfloat16 [512, 512], P(None, 'tp'), may hold values from -0.25 to 0.25
- w_key_up: bfloat16 [512, 1024], P(None, 'tp'), may hold values from -0.25 to 0.25
- w_value_up: bfloat16 [512, 1024], P(None, 'tp'), may hold values from -0.25 to 0.25
- w_branch_window: bfloat16 [1024, 2048], P('tp'), may hold values from -0.1875 to 0.1875
- w_branch_latent: bfloat16 [1024, 2048], P('tp'), may hold values from -0.1875 to 0.1875
- w_gate_window: bfloat16 [2048, 2048], P(None, 'tp'), may hold values from -0.125 to 0.125
- w_gate_latent: bfloat16 [2048, 2048], P(None, 'tp'), may hold values from -0.125 to 0.125
Outputs:
- mixed: bfloat16 [3072, 2048], P('sp', 'tp')
All inputs are finite; a program needn't handle non-finite values.
Results may differ from a plain program's by a relative error of at most 0.018.
The roundings to bfloat16 on the way count: a program that leaves them out, or rounds other values in their place, can miss the bound.
Values may be sent and summed in bfloat16 or wider, within the bound.
A program may use at most 128 MiB of HBM per device.

v0:
```python
import jax
import jax.numpy as jnp
from jax import lax
from jax.sharding import PartitionSpec as P

HEAD = 64
WINDOW = 128
NOPE = 128
ROPE = 64
VDIM = 128
EPS = 1e-06
THETA = 10000.0
NEGATIVE = -1e30


def from_behind(shard, axis, by):
    count = lax.axis_size(axis)
    pairs = [(i, i + by) for i in range(count) if 0 <= i + by < count]
    return lax.ppermute(shard, axis, pairs)


def rms_rows(float_rows, gain_vec):
    return (
        float_rows
        * lax.rsqrt(jnp.mean(float_rows * float_rows, axis=-1, keepdims=True) + EPS)
        * gain_vec
    )


def rotate(float_rows, positions):
    half_width = float_rows.shape[-1] // 2
    frequencies = THETA ** (-jnp.arange(half_width, dtype=jnp.float32) / half_width)
    angles = positions.astype(jnp.float32)[:, None] * frequencies
    target = (float_rows.shape[0],) + (1,) * (float_rows.ndim - 2) + (half_width,)
    cosine = jnp.cos(angles).reshape(target)
    sine_part = jnp.sin(angles).reshape(target)
    first_half = float_rows[..., :half_width]
    second_half = float_rows[..., half_width:]
    return jnp.concatenate(
        [
            first_half * cosine - second_half * sine_part,
            second_half * cosine + first_half * sine_part,
        ],
        axis=-1,
    )


def project(left, right):
    return jnp.dot(left, right, preferred_element_type=jnp.float32)


def window_attention(queries, key_ext, value_ext, sink_table, row_start):
    row_count = queries.shape[0]
    kv_heads = key_ext.shape[1] // HEAD
    group_size = queries.shape[1] // HEAD // kv_heads
    blocks = row_count // WINDOW
    query_blocks = queries.reshape(blocks, WINDOW, kv_heads, group_size, HEAD)

    def banded(table):
        table = table.reshape(blocks + 1, WINDOW, kv_heads, HEAD)
        return jnp.concatenate([table[:-1], table[1:]], axis=1)

    key_band = banded(key_ext)
    value_band = banded(value_ext)
    scores = jnp.einsum(
        "nqhgd,nkhd->nhgqk", query_blocks, key_band, preferred_element_type=jnp.float32
    ) * HEAD ** (-0.5)
    query_index = jnp.arange(WINDOW, dtype=jnp.int32)[:, None]
    key_index = jnp.arange(2 * WINDOW, dtype=jnp.int32)[None, :]
    offset = query_index + WINDOW - key_index
    key_position = (
        row_start + jnp.arange(blocks, dtype=jnp.int32)[:, None, None] * WINDOW + key_index - WINDOW
    )
    valid_mask = ((offset >= 0) & (offset < WINDOW) & (key_position >= 0))[:, None, None]
    scores = jnp.where(valid_mask, scores, NEGATIVE)
    sink_logit = sink_table.reshape(1, kv_heads, group_size, 1, 1)
    row_top = jnp.maximum(jnp.max(scores, axis=-1, keepdims=True), sink_logit)
    weights = jnp.where(valid_mask, jnp.exp(scores - row_top), 0.0)
    denominator = jnp.sum(weights, axis=-1, keepdims=True) + jnp.exp(sink_logit - row_top)
    probabilities = (weights / denominator).astype(jnp.bfloat16)
    attended = jnp.einsum(
        "nhgqk,nkhd->nqhgd", probabilities, value_band, preferred_element_type=jnp.float32
    )
    return attended.astype(jnp.bfloat16).reshape(row_count, kv_heads * group_size * HEAD)


def on_device(
    features,
    norm_gain,
    w_query,
    w_key,
    w_value,
    head_sinks,
    w_query_latent,
    w_kv_latent,
    w_rope_key,
    query_latent_gain,
    kv_latent_gain,
    w_query_content,
    w_query_rotary,
    w_key_up,
    w_value_up,
    w_branch_window,
    w_branch_latent,
    w_gate_window,
    w_gate_latent,
):
    tok_rows = features.shape[0]
    row_start = lax.axis_index("sp") * tok_rows
    row_end = row_start + tok_rows
    positions = row_start + jnp.arange(tok_rows, dtype=jnp.int32)
    gathered = lax.all_gather(features, "tp", axis=1, tiled=True)
    normed = rms_rows(gathered.astype(jnp.float32), norm_gain).astype(jnp.bfloat16)
    query_rows = project(normed, w_query).astype(jnp.bfloat16)
    key_rows = project(normed, w_key).astype(jnp.bfloat16)
    value_rows = project(normed, w_value).astype(jnp.bfloat16)
    key_width = key_rows.shape[1]
    packed = jnp.concatenate([key_rows, value_rows], axis=1)
    tail_rows = from_behind(packed[tok_rows - WINDOW :], "sp", 1)
    extended = jnp.concatenate([tail_rows, packed], axis=0)
    window_out = window_attention(
        query_rows, extended[:, :key_width], extended[:, key_width:], head_sinks, row_start
    )
    latent_query = rms_rows(project(normed, w_query_latent), query_latent_gain).astype(jnp.bfloat16)
    latent_kv = rms_rows(project(normed, w_kv_latent), kv_latent_gain).astype(jnp.bfloat16)
    rope_rows = rotate(project(normed, w_rope_key), positions).astype(jnp.bfloat16)
    lat_heads = w_key_up.shape[1] // NOPE
    query_content = (
        project(latent_query, w_query_content)
        .astype(jnp.bfloat16)
        .reshape(tok_rows, lat_heads, NOPE)
    )
    query_rotary = rotate(
        project(latent_query, w_query_rotary).reshape(tok_rows, lat_heads, ROPE), positions
    ).astype(jnp.bfloat16)
    scale_factor = (NOPE + ROPE) ** (-0.5)

    def attend(running, piece_keys, piece_values, rope_piece):
        running_max, denominator, accumulated = running
        piece_rows = piece_keys.shape[0]
        scores = (
            jnp.einsum(
                "qhd,khd->hqk",
                query_content,
                piece_keys.reshape(piece_rows, lat_heads, NOPE),
                preferred_element_type=jnp.float32,
            )
            + jnp.einsum(
                "qhr,kr->hqk", query_rotary, rope_piece, preferred_element_type=jnp.float32
            )
        ) * scale_factor
        key_position = jnp.arange(piece_rows, dtype=jnp.int32)
        live_mask = key_position[None, :] <= positions[:, None]
        scores = jnp.where(live_mask, scores, NEGATIVE)
        new_max = jnp.maximum(running_max, jnp.max(scores, axis=-1))
        weights = jnp.where(live_mask, jnp.exp(scores - new_max[..., None]), 0.0)
        denominator = jnp.sum(weights, axis=-1)
        accumulated = jnp.einsum(
            "hqk,khd->hqd",
            weights.astype(jnp.bfloat16),
            piece_values.reshape(piece_rows, lat_heads, VDIM),
            preferred_element_type=jnp.float32,
        )
        return (new_max, denominator, accumulated)

    initial = (
        jnp.full((lat_heads, tok_rows), NEGATIVE, jnp.float32),
        jnp.zeros((lat_heads, tok_rows), jnp.float32),
        jnp.zeros((lat_heads, tok_rows, VDIM), jnp.float32),
    )
    pieces = (
        lax.all_gather(latent_kv, "sp", axis=0, tiled=True),
        lax.all_gather(rope_rows, "sp", axis=0, tiled=True),
    )

    def compute(current):
        piece_keys = project(pieces[0], w_key_up).astype(jnp.bfloat16)
        piece_values = project(pieces[0], w_value_up).astype(jnp.bfloat16)
        return attend(current, piece_keys, piece_values, pieces[1])

    running = lax.cond(jnp.int32(0) < row_end, compute, lambda current: current, initial)
    latent_out = jnp.transpose(running[2] / running[1][..., None], (1, 0, 2))
    latent_out = latent_out.reshape(tok_rows, lat_heads * VDIM).astype(jnp.bfloat16)
    all_window, all_latent = (
        lax.all_gather(window_out, "tp", axis=1, tiled=True),
        lax.all_gather(latent_out, "tp", axis=1, tiled=True),
    )
    column_window, column_latent = (
        lax.all_to_all(w_branch_window, "tp", split_axis=1, concat_axis=0, tiled=True),
        lax.all_to_all(w_branch_latent, "tp", split_axis=1, concat_axis=0, tiled=True),
    )
    window_branch = project(all_window, column_window)
    latent_branch = project(all_latent, column_latent)
    window_gate = jax.nn.sigmoid(project(normed, w_gate_window))
    latent_gate = jax.nn.sigmoid(project(normed, w_gate_latent))
    return (window_gate * window_branch + latent_gate * latent_branch).astype(jnp.bfloat16)


def solution(mesh):
    return jax.shard_map(
        on_device,
        mesh=mesh,
        in_specs=(
            P("sp", "tp"),
            P(),
            P(None, "tp"),
            P(None, "tp"),
            P(None, "tp"),
            P("tp"),
            P(),
            P(),
            P(),
            P(),
            P(),
            P(None, "tp"),
            P(None, "tp"),
            P(None, "tp"),
            P(None, "tp"),
            P("tp", None),
            P("tp", None),
            P(None, "tp"),
            P(None, "tp"),
        ),
        out_specs=P("sp", "tp"),
        check_vma=False,
    )
```

profile of v0, /device:TPU:0, one launch (start us, length us, event | category | flops | bytes accessed | tf_op | source)
XLA Modules:
  0.0 168.1 jit_solution(3678124389484324087)
XLA Ops:
  6.5 0.7 all-gather.3.cloned.1.call-update
  7.3 2.3 %copy.60 = bf16[256,2048]{0,1:T(8,128)(2,1)} copy(bf16[256,2048]{1,0:T(8,128)(2,1)} %param.37) | data formatting | bytes 2097152 | tf_op args[16]
  9.5 4.4 %all-to-all-start.1 = ((bf16[256,4,512]{0,2,1:T(8,128)(2,1)}), bf16[256,4,512]{0,2,1:T(8,128)(2,1)S(1)}, u32[]{:S(2)}, u32[]{:S(2)}) async-start(bf16[256,4,512]{0,2,1:T(8,128)(2,1)} %bitcast.96), calls=%async_computation.1 | async-start | bytes 2097152 | tf_op jit(solution)/shard_map/all_to_all | solution.py:190
  14.0 2.3 %copy.57 = bf16[256,2048]{0,1:T(8,128)(2,1)} copy(bf16[256,2048]{1,0:T(8,128)(2,1)} %param.36) | data formatting | bytes 2097152 | tf_op args[15]
  16.3 19.8 %all-to-all-done.1 = bf16[256,4,512]{0,2,1:T(8,128)(2,1)S(1)} async-done(((bf16[256,4,512]{0,2,1:T(8,128)(2,1)}), bf16[256,4,512]{0,2,1:T(8,128)(2,1)S(1)}, u32[]{:S(2)}, u32[]{:S(2)}) %all-to-all-start.1) | async-done | bytes 1048608 | tf_op jit(solution)/shard_map/all_to_all | solution.py:190
  36.1 4.2 %all-to-all-start = ((bf16[256,4,512]{0,2,1:T(8,128)(2,1)}), bf16[256,4,512]{0,2,1:T(8,128)(2,1)}, u32[]{:S(2)}, u32[]{:S(2)}) async-start(bf16[256,4,512]{0,2,1:T(8,128)(2,1)} %bitcast.97), calls=%async_computation | async-start | bytes 2097152 | tf_op jit(solution)/shard_map/all_to_all | solution.py:189
  40.7 1.3 copy.61
  42.0 12.8 %all-to-all-done = bf16[256,4,512]{0,2,1:T(8,128)(2,1)} async-done(((bf16[256,4,512]{0,2,1:T(8,128)(2,1)}), bf16[256,4,512]{0,2,1:T(8,128)(2,1)}, u32[]{:S(2)}, u32[]{:S(2)}) %all-to-all-start) | async-done | bytes 1048608 | tf_op jit(solution)/shard_map/all_to_all | solution.py:189
  54.8 2.3 %copy.58 = bf16[4,256,512]{2,1,0:T(8,128)(2,1)} copy(bf16[4,256,512]{1,2,0:T(8,128)(2,1)} %bitcast.12) | data formatting | bytes 2097152 | tf_op jit(solution)/shard_map/all_to_all | solution.py:189
  57.1 1.9 %fusion.14 = f32[384]{0:T(512)S(1)} fusion(bf16[384,2048]{1,0:T(8,128)(2,1)} %all-gather.3.cloned.1.call-done), kind=kLoop, calls=%fused_computation.22 | loop fusion | flops 2358912 | bytes 1574400 | tf_op jit(solution)/shard_map/reduce_sum | solution.py:25
  59.1 0.4 fusion.16
  59.5 1.1 multiply_reduce_fusion.1
  60.7 0.9 multiply_convert_fusion.1
  61.7 2.0 %convolution_convert_fusion.6 = bf16[384,128]{0,1:T(8,128)(2,1)S(1)} fusion(bf16[384,2048]{1,0:T(8,128)(2,1)} %copy-done.2, bf16[2048,128]{1,0:T(8,128)(2,1)S(1)} %copy-done.12), kind=kOutput, calls=%fused_computation.46 | convolution fusion | flops 201375744 | bytes 2195456 | tf_op jit(solution)/shard_map/dot_general | solution.py:49
  63.8 2.0 %convolution_convert_fusion.5 = bf16[384,128]{0,1:T(8,128)(2,1)S(1)} fusion(bf16[384,2048]{1,0:T(8,128)(2,1)} %copy-done.2, bf16[2048,128]{1,0:T(8,128)(2,1)S(1)} %copy-done.13), kind=kOutput, calls=%fused_computation.45 | convolution fusion | flops 201375744 | bytes 2195456 | tf_op jit(solution)/shard_map/dot_general | solution.py:49
  65.8 0.6 pad_maximum_fusion.4
  66.5 5.2 %collective-permute-start = (bf16[128,256]{0,1:T(8,128)(2,1)}, bf16[128,256]{0,1:T(8,128)(2,1)}, u32[]{:S(2)}, u32[]{:S(2)}) collective-permute-start(bf16[128,256]{0,1:T(8,128)(2,1)} %pad_maximum_fusion.4), channel_id=1, source_target_pairs={{0,4},{4,8},{8,12},{12,16},{16,20},{20,24},{24,28},{1,5},{5,9},{9,... | collective-permute-start | bytes 196616 | tf_op jit(solution)/shard_map/ppermute | solution.py:19
  71.7 0.6 copy.52
  72.3 2.3 %convolution_convert_fusion.3 = bf16[384,256]{1,0:T(8,128)(2,1)S(1)} fusion(bf16[384,2048]{1,0:T(8,128)(2,1)} %copy-done.2, bf16[2048,256]{1,0:T(8,128)(2,1)} %param.23), kind=kOutput, calls=%fused_computation.42 | convolution fusion | flops 402751488 | bytes 2818048 | tf_op jit(solution)/shard_map/dot_general | solution.py:49
  74.7 0.2 reshape.210
  74.9 2.1 %fusion.41 = f32[384,64]{0,1:T(8,128)S(1)} fusion(bf16[384,2048]{1,0:T(8,128)(2,1)} %copy-done.2, bf16[2048,64]{0,1:T(8,128)(2,1)S(1)} %copy-done.18), kind=kOutput, calls=%fused_computation.93 | convolution fusion | flops 100663296 | bytes 1933312 | tf_op jit(solution)/shard_map/dot_general | solution.py:49
  77.0 0.3 multiply_cosine_fusion
  77.3 35.1 %all_gather.18 = bf16[3072,64]{0,1:T(8,128)(2,1)} all-gather(bf16[384,64]{0,1:T(8,128)(2,1)S(1)} %pad_maximum_fusion.5), channel_id=1, replica_groups=mesh['sp'=8,'tp'=4] {'sp'}, dimensions={0}, use_global_device_ids=true | all-gather | bytes 442368 | tf_op jit(solution)/shard_map/all_gather | solution.py:173
  112.5 2.7 %multiply_reduce_fusion = (f32[384]{0:T(512)S(1)}, f32[384,512]{1,0:T(8,128)S(1)}) fusion(bf16[384,2048]{1,0:T(8,128)(2,1)S(1)} %copy-done.3, bf16[2048,512]{1,0:T(8,128)(2,1)} %param.27), kind=kOutput, calls=%fused_computation.48 | convolution fusion | flops 805699200 | bytes 4457984 | tf_op jit(solution)/shard_map/dot_general | solution.py:49
  115.2 0.4 fusion.38
  115.6 0.5 copy-done.15
  116.1 1.0 convolution_convert_fusion.2
  117.1 2.0 %fusion.24 = f32[384,512]{1,0:T(8,128)} fusion(bf16[384,2048]{1,0:T(8,128)(2,1)S(1)} %copy-done.3, bf16[2048,512]{1,0:T(8,128)(2,1)S(1)} %copy-done.24), kind=kOutput, calls=%fused_computation.39 | convolution fusion | flops 805896192 | bytes 4456448 | tf_op jit(solution)/shard_map/dot_general | solution.py:49
  119.1 2.0 %fusion.22 = f32[384,512]{1,0:T(8,128)} fusion(bf16[384,2048]{1,0:T(8,128)(2,1)S(1)} %copy-done.3, bf16[2048,512]{1,0:T(8,128)(2,1)S(1)} %copy-done.25), kind=kOutput, calls=%fused_computation.37 | convolution fusion | flops 805896192 | bytes 4456448 | tf_op jit(solution)/shard_map/dot_general | solution.py:49
  121.0 0.6 pad_maximum_fusion.3
  121.7 0.8 pad_maximum_fusion.2
  122.6 0.4 fusion.40
  123.1 0.3 fusion.20
  123.5 0.5 fusion.26
  124.0 0.2 copy.56
  124.3 7.9 %all_gather.16 = bf16[384,1024]{0,1:T(8,128)(2,1)} all-gather(bf16[384,256]{0,1:T(8,128)(2,1)S(1)} %bitcast.100), channel_id=1, replica_groups=mesh['sp'=8,'tp'=4] {'tp'}, dimensions={1}, use_global_device_ids=true | all-gather | bytes 983040 | tf_op jit(solution)/shard_map/all_gather | solution.py:185
  132.2 15.7 %conditional.1 = (f32[2,384]{1,0:T(2,128)S(1)}, f32[2,384,128]{1,2,0:T(8,128)}) conditional(s32[]{:T(128)} %convert_element_type.75, () %tuple.13, (s32[]{:T(128)}, s32[384]{0:T(512)S(1)}, bf16[3072,512]{1,0:T(8,128)(2,1)}, bf16[512,256]{1,0:T(8,128)(2,1)S(1)}, bf16[384,256]{1,0:T(8,128)(2,1)}, /*index=5*/bf16[3072,64]{0,1:T(8,128)(2,1)}, ...), branch_computations={%region_5.6_spmd, %region_6.9_spmd} | conditional | flops 3146907136 | bytes 87218872 | solution.py:181
  132.2 0.9 iota_compare_fusion
  133.1 3.4 %convolution_convert_fusion.1 = bf16[3072,256]{0,1:T(8,128)(2,1)S(1)} fusion(bf16[3072,512]{1,0:T(8,128)(2,1)} %get-tuple-element.26, bf16[512,256]{1,0:T(8,128)(2,1)S(1)} %get-tuple-element.38), kind=kOutput, calls=%fused_computation.12 | convolution fusion | flops 806092800 | bytes 4980736 | tf_op jit(solution)/shard_map/cond/branch_1_fun/dot_general | solution.py:49
  136.5 1.6 fusion.10
  138.1 2.4 %fusion.39 = (f32[2,384]{1,0:T(2,128)S(1)}, f32[2,384,3072]{1,2,0:T(8,128)S(1)}) fusion(bf16[384,2,64]{0,2,1:T(8,128)(2,1)S(1)} %copy-done.14, bf16[3072,64]{0,1:T(8,128)(2,1)S(1)} %copy-done.9, f32[2,3072,384]{2,1,0:T(8,128)S(1)} %fusion.10, pred[384,3072]{0,1:T(8,128)(4,1)S(1)} %iota_compare_fusion), kind=kOutput, calls=%fused_computation.91 | convolution fusion | flops 311426304 | bytes 20548608 | tf_op jit(solution)/shard_map/cond/branch_1_fun/qhr,kr->hqk/dot_general | solution.py:148
  140.5 1.0 convolution_convert_fusion
  141.6 3.1 %fusion.4 = f32[2,384,128]{1,2,0:T(8,128)} fusion(bf16[3072,2,128]{0,2,1:T(8,128)(2,1)S(1)} %bitcast.93, f32[2,384,3072]{1,2,0:T(8,128)S(1)} %get-tuple-element.42, f32[2,384]{1,0:T(2,128)S(1)} %broadcast_maximum_fusion, pred[384,3072]{0,1:T(8,128)(4,1)S(1)} %iota_compare_fusion), kind=kOutput, calls=%fused_computation.6 | convolution fusion | flops 611057664 | bytes 12585984 | tf_op jit(solution)/shard_map/cond | solution.py:181
  144.7 3.2 %fusion.3 = f32[2,384]{1,0:T(2,128)S(1)} fusion(f32[2,384,3072]{1,2,0:T(8,128)S(1)} %get-tuple-element.42, f32[2,384]{1,0:T(2,128)S(1)} %broadcast_maximum_fusion, pred[384,3072]{0,1:T(8,128)(4,1)} %copy-done.4), kind=kLoop, calls=%fused_computation.5 | loop fusion | flops 7077120 | bytes 10622976 | tf_op jit(solution)/shard_map/cond/branch_1_fun/reduce_sum | solution.py:157
  147.9 1.1 divide_convert_fusion.2
  149.0 9.0 %all_gather.19 = bf16[384,1024]{0,1:T(8,128)(2,1)S(1)} all-gather(bf16[384,256]{0,1:T(8,128)(2,1)S(1)} %bitcast.102), channel_id=1, replica_groups=mesh['sp'=8,'tp'=4] {'tp'}, dimensions={1}, use_global_device_ids=true | all-gather | bytes 983040 | tf_op jit(solution)/shard_map/all_gather | solution.py:186
  158.0 1.9 %convolution_multiply_fusion = f32[384,512]{1,0:T(8,128)S(1)} fusion(f32[384,512]{1,0:T(8,128)} %fusion.24, bf16[384,1024]{0,1:T(8,128)(2,1)S(1)} %all_gather.19, bf16[1024,512]{1,0:T(8,128)(2,1)S(1)} %bitcast.94), kind=kOutput, calls=%fused_computation.28 | convolution fusion | flops 402849792 | bytes 3407872 | tf_op jit(solution)/shard_map/dot_general | solution.py:49
  159.9 1.4 fusion.25
  (85 shorter events, 1.2 us)
Async XLA Ops:
  6.5 53.0 %copy-start = (bf16[2048,512]{1,0:T(8,128)(2,1)S(1)}, bf16[2048,512]{1,0:T(8,128)(2,1)}, u32[]{:S(2)}) copy-start(bf16[2048,512]{1,0:T(8,128)(2,1)} %param.28) | copy-start | bytes 6291460
  6.5 50.6 %all-gather.3.cloned.1.call-start = ((), (), s32[]{:S(2)}) async-start(), calls=%async_computation.2 | async-start | bytes 1966080 | tf_op jit(solution)/shard_map/all_gather | solution.py:112
  9.5 4.4 %copy-start.26 = (f32[4]{0:T(128)S(1)}, f32[4]{0:T(128)}, u32[]{:S(2)}) copy-start(f32[4]{0:T(128)} %param.26) | copy-start | bytes 52
  9.5 26.6 %all-to-all-start.1 = ((bf16[256,4,512]{0,2,1:T(8,128)(2,1)}), bf16[256,4,512]{0,2,1:T(8,128)(2,1)S(1)}, u32[]{:S(2)}, u32[]{:S(2)}) async-start(bf16[256,4,512]{0,2,1:T(8,128)(2,1)} %bitcast.96), calls=%async_computation.1 | async-start | bytes 2097152 | tf_op jit(solution)/shard_map/all_to_all | solution.py:190
  36.1 18.7 %all-to-all-start = ((bf16[256,4,512]{0,2,1:T(8,128)(2,1)}), bf16[256,4,512]{0,2,1:T(8,128)(2,1)}, u32[]{:S(2)}, u32[]{:S(2)}) async-start(bf16[256,4,512]{0,2,1:T(8,128)(2,1)} %bitcast.97), calls=%async_computation | async-start | bytes 2097152 | tf_op jit(solution)/shard_map/all_to_all | solution.py:189
  40.3 91.8 %all-gather.5.cloned.1.call-start = ((), (), s32[]{:S(2)}) async-start(), calls=%async_computation.3 | async-start | bytes 3538944 | tf_op jit(solution)/shard_map/all_gather | solution.py:172
  54.8 4.2 %copy-start.21 = (f32[2048]{0:T(1024)S(1)}, f32[2048]{0:T(1024)}, u32[]{:S(2)}) copy-start(f32[2048]{0:T(1024)} %param.22) | copy-start | bytes 24580
  57.1 1.9 %copy-start.5 = (bf16[384,2048]{1,0:T(8,128)(2,1)S(1)}, bf16[384,2048]{1,0:T(8,128)(2,1)}, u32[]{:S(2)}) copy-start(bf16[384,2048]{1,0:T(8,128)(2,1)} %all-gather.3.cloned.1.call-done) | copy-start | bytes 4718596
  59.5 1.2 copy-start.2
  59.5 1.2 copy-start.23
  60.7 1.0 copy-start.12
  61.6 2.2 %copy-start.13 = (bf16[2048,128]{1,0:T(8,128)(2,1)S(1)}, bf16[2048,128]{1,0:T(8,128)(2,1)}, u32[]{:S(2)}) copy-start(bf16[2048,128]{1,0:T(8,128)(2,1)} %param.25) | copy-start | bytes 1572868
  66.5 55.2 %collective-permute-start = (bf16[128,256]{0,1:T(8,128)(2,1)}, bf16[128,256]{0,1:T(8,128)(2,1)}, u32[]{:S(2)}, u32[]{:S(2)}) collective-permute-start(bf16[128,256]{0,1:T(8,128)(2,1)} %pad_maximum_fusion.4), channel_id=1, source_target_pairs={{0,4},{4,8},{8,12},{12,16},{16,20},{20,24},{24,28},{1,5},{5,9},{9,... | collective-permute-start | bytes 196616 | tf_op jit(solution)/shard_map/ppermute | solution.py:19
  72.3 2.6 %copy-start.18 = (bf16[2048,64]{0,1:T(8,128)(2,1)S(1)}, bf16[2048,64]{0,1:T(8,128)(2,1)}, u32[]{:S(2)}) copy-start(bf16[2048,64]{0,1:T(8,128)(2,1)} %param.29) | copy-start | bytes 786436
  74.9 37.6 %copy-start.3 = (bf16[384,2048]{1,0:T(8,128)(2,1)S(1)}, bf16[384,2048]{1,0:T(8,128)(2,1)}, u32[]{:S(2)}) copy-start(bf16[384,2048]{1,0:T(8,128)(2,1)} %copy-done.2) | copy-start | bytes 4718596
  112.4 2.7 %copy-start.19 = (bf16[512,128]{1,0:T(8,128)(2,1)S(1)}, bf16[512,128]{1,0:T(8,128)(2,1)}, u32[]{:S(2)}) copy-start(bf16[512,128]{1,0:T(8,128)(2,1)} %param.33) | copy-start | bytes 393220
  112.4 2.7 %copy-start.22 = (f32[512]{0:T(512)S(1)}, f32[512]{0:T(512)}, u32[]{:S(2)}) copy-start(f32[512]{0:T(512)} %param.30) | copy-start | bytes 6148
  115.1 1.0 copy-start.15
  115.1 1.9 %copy-start.24 = (bf16[2048,512]{1,0:T(8,128)(2,1)S(1)}, bf16[2048,512]{1,0:T(8,128)(2,1)}, u32[]{:S(2)}) copy-start(bf16[2048,512]{1,0:T(8,128)(2,1)} %param.39) | copy-start | bytes 6291460
  117.1 2.0 %copy-start.25 = (bf16[2048,512]{1,0:T(8,128)(2,1)S(1)}, bf16[2048,512]{1,0:T(8,128)(2,1)}, u32[]{:S(2)}) copy-start(bf16[2048,512]{1,0:T(8,128)(2,1)} %param.38) | copy-start | bytes 6291460
  121.0 1.6 copy-start.20
  124.0 8.1 %copy-start.16 = (bf16[512,256]{1,0:T(8,128)(2,1)S(1)}, bf16[512,256]{1,0:T(8,128)(2,1)}, u32[]{:S(2)}) copy-start(bf16[512,256]{1,0:T(8,128)(2,1)} %param.34) | copy-start | bytes 786436
  133.1 8.5 %copy-start.4 = (pred[384,3072]{0,1:T(8,128)(4,1)}, pred[384,3072]{0,1:T(8,128)(4,1)S(1)}, u32[]{:S(2)}) copy-start(pred[384,3072]{0,1:T(8,128)(4,1)S(1)} %iota_compare_fusion) | copy-start | bytes 3538948 | tf_op jit(solution)/shard_map/cond
  133.1 3.4 %copy-start.11 = (bf16[384,256]{1,0:T(8,128)(2,1)S(1)}, bf16[384,256]{1,0:T(8,128)(2,1)}, u32[]{:S(2)}) copy-start(bf16[384,256]{1,0:T(8,128)(2,1)} %get-tuple-element.28) | copy-start | bytes 589828 | tf_op jit(solution)/shard_map/cond
  136.5 1.6 copy-start.9
  136.5 1.6 copy-start.14
  138.1 2.5 %copy-start.1 = (bf16[3072,512]{1,0:T(8,128)(2,1)S(1)}, bf16[3072,512]{1,0:T(8,128)(2,1)}, u32[]{:S(2)}) copy-start(bf16[3072,512]{1,0:T(8,128)(2,1)} %get-tuple-element.26) | copy-start | bytes 9437188 | tf_op jit(solution)/shard_map/cond
  138.1 2.5 %copy-start.17 = (bf16[512,256]{1,0:T(8,128)(2,1)S(1)}, bf16[512,256]{1,0:T(8,128)(2,1)}, u32[]{:S(2)}) copy-start(bf16[512,256]{1,0:T(8,128)(2,1)} %get-tuple-element.39) | copy-start | bytes 786436 | tf_op jit(solution)/shard_map/cond
  147.9 10.1 %copy-start.6 = (bf16[4,256,512]{2,1,0:T(8,128)(2,1)S(1)}, bf16[4,256,512]{2,1,0:T(8,128)(2,1)}, u32[]{:S(2)}) copy-start(bf16[4,256,512]{2,1,0:T(8,128)(2,1)} %copy.61) | copy-start | bytes 3145732
  158.0 1.9 %copy-start.7 = (bf16[4,256,512]{2,1,0:T(8,128)(2,1)S(1)}, bf16[4,256,512]{2,1,0:T(8,128)(2,1)}, u32[]{:S(2)}) copy-start(bf16[4,256,512]{2,1,0:T(8,128)(2,1)} %copy.58) | copy-start | bytes 3145732
  158.0 1.9 %copy-start.8 = (bf16[384,1024]{0,1:T(8,128)(2,1)S(1)}, bf16[384,1024]{0,1:T(8,128)(2,1)}, u32[]{:S(2)}) copy-start(bf16[384,1024]{0,1:T(8,128)(2,1)} %all_gather.16) | copy-start | bytes 2359300
  158.0 1.9 %copy-start.10 = (f32[384,512]{1,0:T(8,128)S(1)}, f32[384,512]{1,0:T(8,128)}, u32[]{:S(2)}) copy-start(f32[384,512]{1,0:T(8,128)} %fusion.22) | copy-start | bytes 2359300
Sparse Core Ops, SparseCore 0:
  8.9 29.3 all-gather.2
  61.7 65.5 all-gather.4
where the time goes:
time: 169 us; the launch traced here: 168 us
  blocking collectives  52 us (31%)
  waiting for transfers between devices  33.3 us (20%)
  matrix products  33.2 us (20%)
  starting transfers between devices  13.9 us (8%)
  between operations  13.7 us (8%)
  other arithmetic  11.6 us (7%)
  local copies, waits for them, and re-layouts  10.3 us (6%)
    all_gather x1, blocking collectives, on_device(): lax.all_gather(rope_rows, 'sp', axis=0, tiled=True)  35.1 us
    dot_general x14, matrix products, project(): return jnp.dot(left, right, preferred_element_type=jnp.float32)  25.1 us
    all_to_all x1, waiting for transfers between devices, on_device(): lax.all_to_all(w_branch_latent, 'tp', split_axis=1, concat_axis=0, tiled=...  19.8 us
    all_to_all x1, waiting for transfers between devices, on_device(): lax.all_to_all(w_branch_window, 'tp', split_axis=1, concat_axis=0, tiled=...  12.8 us
    all_gather x1, blocking collectives, on_device(): lax.all_gather(latent_out, 'tp', axis=1, tiled=True)  8.98 us
    all_gather x1, blocking collectives, on_device(): lax.all_gather(window_out, 'tp', axis=1, tiled=True)  7.89 us
    unnamed x45, local copies, waits for them, and re-layouts  5.36 us
    ppermute x1, starting transfers between devices, from_behind(): return lax.ppermute(shard, axis, pairs)  5.23 us
  transfers between devices with their start and end apart: 5, of which 2 were waited for; matrix products, arithmetic and copies ran while one was open for 18% of the time, Pallas kernels for 0%

commit v1 on v0

--- a/solution.py
+++ b/solution.py
@@ -183,7 +183,7 @@
     latent_out = latent_out.reshape(tok_rows, lat_heads * VDIM).astype(jnp.bfloat16)
     all_window, all_latent = (
         lax.all_gather(window_out, "tp", axis=1, tiled=True),
-        lax.all_gather(latent_out, "tp", axis=1, tiled=True),
+        jnp.concatenate(lax.all_gather(latent_out, "tp"), axis=1),
     )
     column_window, column_latent = (
         lax.all_to_all(w_branch_window, "tp", split_axis=1, concat_axis=0, tiled=True),

time: 169 us -> 160 us (0.947)
  waiting for transfers between devices: 33.3 us -> 17.3 us
  local copies, waits for them, and re-layouts: 10.3 us -> 17 us
  other arithmetic: 11.6 us -> 9.37 us
  matrix products: 33.2 us -> 35 us
  blocking collectives: 52 us -> 53.8 us
    all_to_all x1, waiting for transfers between devices: 19.8 us -> 0.01 us  [on_device(): lax.all_to_all(w_branch_latent, 'tp', split_axis=1, concat_axis=0, tiled=...]
    all_to_all x1, waiting for transfers between devices: 12.8 us -> 16.6 us  [on_device(): lax.all_to_all(w_branch_window, 'tp', split_axis=1, concat_axis=0, tiled=...]
    dot_general x0 -> x1, matrix products: none -> 3.25 us  [attend(): jnp.einsum('hqk,khd->hqd', weights.astype(jnp.bfloat16), piece_values.res...]
    cond x1 -> x0, matrix products: 3.14 us -> none  [on_device(): lax.cond(jnp.int32(0) < row_end, compute, lambda current: current, initial)]
    slice x8, local copies, waits for them, and re-layouts: 0.83 us -> 3.69 us  [banded(): return jnp.concatenate([table[:-1], table[1:]], axis=1)]
    all_gather x1, blocking collectives: 7.89 us -> 9.62 us  [on_device(): lax.all_gather(window_out, 'tp', axis=1, tiled=True)]
    reshape x1, local copies, waits for them, and re-layouts: 0.2 us -> 1.91 us  [window_attention(): query_blocks = queries.reshape(blocks, WINDOW, kv_heads, group_size, HEAD)]
    unnamed x45 -> x39, local copies, waits for them, and re-layouts: 5.36 us -> 6.21 us
  transfers between devices with their start and end apart: 5 -> 5, of which waited for: 2 -> 1; matrix products, arithmetic and copies ran while one was open for 18% -> 35% of each run, Pallas kernels for 0% -> 0%
where the time goes in v1:
time: 160 us
  blocking collectives  53.8 us (34%)
  matrix products  35 us (22%)
  waiting for transfers between devices  17.3 us (11%)
  local copies, waits for them, and re-layouts  17 us (11%)
  between operations  13.7 us (9%)
  starting transfers between devices  13.2 us (8%)
  other arithmetic  9.37 us (6%)
    all_gather x1, blocking collectives, on_device(): lax.all_gather(rope_rows, 'sp', axis=0, tiled=True)  35 us
    dot_general x14, matrix products, project(): return jnp.dot(left, right, preferred_element_type=jnp.float32)  25.8 us
    all_to_all x1, waiting for transfers between devices, on_device(): lax.all_to_all(w_branch_window, 'tp', split_axis=1, concat_axis=0, tiled=...  16.6 us
    all_gather x1, blocking collectives, on_device(): lax.all_gather(window_out, 'tp', axis=1, tiled=True)  9.62 us
    all_gather x1, blocking collectives, on_device(): lax.all_gather(latent_out, 'tp')  9.16 us
    unnamed x39, local copies, waits for them, and re-layouts  6.21 us
    ppermute x1, starting transfers between devices, from_behind(): return lax.ppermute(shard, axis, pairs)  5.24 us
    all_to_all x1, starting transfers between devices, on_device(): lax.all_to_all(w_branch_window, 'tp', split_axis=1, concat_axis=0, tiled=...  4.4 us
  transfers between devices with their start and end apart: 5, of which 1 were waited for; matrix products, arithmetic and copies ran while one was open for 35% of the time, Pallas kernels for 0%

profile of v1, /device:TPU:0, one launch (start us, length us, event | category | flops | bytes accessed | tf_op | source)
XLA Modules:
  0.0 159.5 jit_solution(5919487533344396692)
XLA Ops:
  6.5 0.7 all-gather.3.cloned.1.call-update
  7.3 2.3 %copy.77 = bf16[256,2048]{0,1:T(8,128)(2,1)} copy(bf16[256,2048]{1,0:T(8,128)(2,1)} %param.36) | data formatting | bytes 2097152 | tf_op args[15]
  9.5 4.4 %all-to-all-start = ((bf16[256,4,512]{0,2,1:T(8,128)(2,1)}), bf16[256,4,512]{0,2,1:T(8,128)(2,1)S(1)}, u32[]{:S(2)}, u32[]{:S(2)}) async-start(bf16[256,4,512]{0,2,1:T(8,128)(2,1)} %bitcast.100), calls=%async_computation | async-start | bytes 2097152 | tf_op jit(solution)/shard_map/all_to_all | solution.py:189
  14.0 2.3 %copy.80 = bf16[256,2048]{0,1:T(8,128)(2,1)} copy(bf16[256,2048]{1,0:T(8,128)(2,1)} %param.37) | data formatting | bytes 2097152 | tf_op args[16]
  16.3 2.3 %copy.81 = bf16[256,4,512]{2,0,1:T(8,128)(2,1)} copy(bf16[256,4,512]{0,2,1:T(8,128)(2,1)} %bitcast.101) | data formatting | bytes 2097152 | tf_op jit(solution)/shard_map/all_to_all | solution.py:190
  18.7 0.8 broadcast_and_fusion
  19.5 16.6 %all-to-all-done = bf16[256,4,512]{0,2,1:T(8,128)(2,1)S(1)} async-done(((bf16[256,4,512]{0,2,1:T(8,128)(2,1)}), bf16[256,4,512]{0,2,1:T(8,128)(2,1)S(1)}, u32[]{:S(2)}, u32[]{:S(2)}) %all-to-all-start) | async-done | bytes 1048608 | tf_op jit(solution)/shard_map/all_to_all | solution.py:189
  36.1 1.0 copy-done.5
  37.0 3.5 %all-to-all-start.1 = ((bf16[256,4,512]{2,0,1:T(8,128)(2,1)}), bf16[256,4,512]{2,0,1:T(8,128)(2,1)S(1)}, u32[]{:S(2)}, u32[]{:S(2)}) async-start(bf16[256,4,512]{2,0,1:T(8,128)(2,1)} %copy.81), calls=%async_computation.1 | async-start | bytes 2097152 | tf_op jit(solution)/shard_map/all_to_all | solution.py:190
  40.6 2.3 %copy.78 = bf16[4,256,512]{2,1,0:T(8,128)(2,1)} copy(bf16[4,256,512]{1,2,0:T(8,128)(2,1)} %bitcast.99) | data formatting | bytes 2097152 | tf_op jit(solution)/shard_map/all_to_all | solution.py:189
  42.9 1.9 %fusion.14 = f32[384]{0:T(512)S(1)} fusion(bf16[384,2048]{1,0:T(8,128)(2,1)} %all-gather.3.cloned.1.call-done), kind=kLoop, calls=%fused_computation.22 | loop fusion | flops 2358912 | bytes 1574400 | tf_op jit(solution)/shard_map/reduce_sum | solution.py:25
  44.8 0.4 fusion.16
  45.3 1.1 multiply_reduce_fusion.1
  46.5 0.9 multiply_convert_fusion.1
  47.4 2.1 %convolution_convert_fusion.6 = bf16[384,128]{0,1:T(8,128)(2,1)S(1)} fusion(bf16[384,2048]{1,0:T(8,128)(2,1)} %copy-done.2, bf16[2048,128]{1,0:T(8,128)(2,1)} %param.24), kind=kOutput, calls=%fused_computation.47 | convolution fusion | flops 201375744 | bytes 2195456 | tf_op jit(solution)/shard_map/dot_general | solution.py:49
  49.5 0.7 slice.49
  50.2 2.1 %convolution_convert_fusion.5 = bf16[384,128]{0,1:T(8,128)(2,1)S(1)} fusion(bf16[384,2048]{1,0:T(8,128)(2,1)} %copy-done.2, bf16[2048,128]{1,0:T(8,128)(2,1)} %param.25), kind=kOutput, calls=%fused_computation.46 | convolution fusion | flops 201375744 | bytes 2195456 | tf_op jit(solution)/shard_map/dot_general | solution.py:49
  52.3 5.2 %collective-permute-start = (bf16[128,256]{0,1:T(8,128)(2,1)S(1)}, bf16[128,256]{0,1:T(8,128)(2,1)}, u32[]{:S(2)}, u32[]{:S(2)}) collective-permute-start(bf16[128,256]{0,1:T(8,128)(2,1)S(1)} %pad_maximum_fusion.4), channel_id=1, source_target_pairs={{0,4},{4,8},{8,12},{12,16},{16,20},{20,24},{24,28},{1,5},{5,9},{9,... | collective-permute-start | bytes 196616 | tf_op jit(solution)/shard_map/ppermute | solution.py:19
  57.6 1.6 copy.72
  59.1 3.0 %convolution_convert_fusion.3 = bf16[384,256]{1,0:T(8,128)(2,1)} fusion(bf16[384,2048]{1,0:T(8,128)(2,1)} %copy-done.2, bf16[2048,256]{1,0:T(8,128)(2,1)} %param.23), kind=kOutput, calls=%fused_computation.43 | convolution fusion | flops 402751488 | bytes 2818048 | tf_op jit(solution)/shard_map/dot_general | solution.py:49
  62.1 1.9 %reshape.226 = bf16[3,128,2,2,64]{4,3,2,1,0:T(2,128)(2,1)} reshape(bf16[384,256]{1,0:T(8,128)(2,1)} %convolution_convert_fusion.3) | data formatting | bytes 393216 | tf_op jit(solution)/shard_map/reshape | solution.py:57
  64.1 0.7 copy.70
  64.7 2.0 %fusion.45 = f32[384,64]{0,1:T(8,128)S(1)} fusion(bf16[384,2048]{1,0:T(8,128)(2,1)} %copy-done.2, bf16[2048,64]{0,1:T(8,128)(2,1)} %param.29), kind=kOutput, calls=%fused_computation.97 | convolution fusion | flops 100663296 | bytes 1933312 | tf_op jit(solution)/shard_map/dot_general | solution.py:49
  67.0 35.0 %all_gather.19 = bf16[3072,64]{0,1:T(8,128)(2,1)} all-gather(bf16[384,64]{0,1:T(8,128)(2,1)S(1)} %pad_maximum_fusion.5), channel_id=1, replica_groups=mesh['sp'=8,'tp'=4] {'sp'}, dimensions={0}, use_global_device_ids=true | all-gather | bytes 442368 | tf_op jit(solution)/shard_map/all_gather | solution.py:173
  102.1 2.7 %multiply_reduce_fusion = (f32[384]{0:T(512)S(1)}, f32[384,512]{1,0:T(8,128)S(1)}) fusion(bf16[384,2048]{1,0:T(8,128)(2,1)S(1)} %copy-done.3, bf16[2048,512]{1,0:T(8,128)(2,1)} %param.27), kind=kOutput, calls=%fused_computation.51 | convolution fusion | flops 805699200 | bytes 4457984 | tf_op jit(solution)/shard_map/dot_general | solution.py:49
  104.8 0.4 fusion.42
  105.3 0.5 copy-done.13
  105.8 1.0 convolution_convert_fusion.2
  106.8 2.0 %fusion.25 = f32[384,512]{1,0:T(8,128)} fusion(bf16[384,2048]{1,0:T(8,128)(2,1)S(1)} %copy-done.3, bf16[2048,512]{1,0:T(8,128)(2,1)S(1)} %copy-done.20), kind=kOutput, calls=%fused_computation.40 | convolution fusion | flops 805896192 | bytes 4456448 | tf_op jit(solution)/shard_map/dot_general | solution.py:49
  108.8 2.0 %fusion.23 = f32[384,512]{1,0:T(8,128)} fusion(bf16[384,2048]{1,0:T(8,128)(2,1)S(1)} %copy-done.3, bf16[2048,512]{1,0:T(8,128)(2,1)S(1)} %copy-done.21), kind=kOutput, calls=%fused_computation.38 | convolution fusion | flops 805896192 | bytes 4456448 | tf_op jit(solution)/shard_map/dot_general | solution.py:49
  110.8 0.7 pad_maximum_fusion.3
  111.4 0.8 pad_maximum_fusion.2
  112.3 0.6 copy.71
  113.0 1.6 fusion.44
  114.6 0.3 fusion.21
  115.1 0.5 fusion.27
  115.8 9.6 %all_gather.17 = bf16[384,1024]{0,1:T(8,128)(2,1)} all-gather(bf16[384,256]{0,1:T(8,128)(2,1)S(1)} %bitcast.104), channel_id=1, replica_groups=mesh['sp'=8,'tp'=4] {'tp'}, dimensions={1}, use_global_device_ids=true | all-gather | bytes 983040 | tf_op jit(solution)/shard_map/all_gather | solution.py:185
  125.4 14.1 %conditional.1 = (f32[2,384]{1,0:T(2,128)S(1)}, f32[2,384,128]{2,1,0:T(8,128)S(1)}) conditional(s32[]{:T(128)} %convert_element_type.82, () %tuple.13, (s32[]{:T(128)}, s32[384]{0:T(512)S(1)}, bf16[3072,512]{1,0:T(8,128)(2,1)}, bf16[512,256]{1,0:T(8,128)(2,1)}, bf16[384,256]{1,0:T(8,128)(2,1)}, /*index=5*/bf16[3072,64]{0,1:T(8,128)(2,1)}, ...), branch_computations={%region_5.6_spmd, %region_6.9_spmd} | conditional | flops 3146907136 | bytes 82500256 | solution.py:181
  125.4 0.9 iota_compare_fusion
  126.3 3.0 %convolution_convert_fusion.1 = bf16[3072,256]{0,1:T(8,128)(2,1)S(1)} fusion(bf16[3072,512]{1,0:T(8,128)(2,1)} %get-tuple-element.26, bf16[512,256]{1,0:T(8,128)(2,1)} %get-tuple-element.38), kind=kOutput, calls=%fused_computation.12 | convolution fusion | flops 806092800 | bytes 4980736 | tf_op jit(solution)/shard_map/cond/branch_1_fun/dot_general | solution.py:49
  129.3 1.6 fusion.10
  130.9 2.4 %fusion.43 = (f32[2,384]{1,0:T(2,128)S(1)}, f32[2,384,3072]{1,2,0:T(8,128)S(1)}) fusion(bf16[384,2,64]{0,2,1:T(8,128)(2,1)S(1)} %copy-done.11, bf16[3072,64]{0,1:T(8,128)(2,1)S(1)} %copy-done.8, f32[2,3072,384]{2,1,0:T(8,128)S(1)} %fusion.10, pred[384,3072]{0,1:T(8,128)(4,1)S(1)} %iota_compare_fusion), kind=kOutput, calls=%fused_computation.95 | convolution fusion | flops 311426304 | bytes 20548608 | tf_op jit(solution)/shard_map/cond/branch_1_fun/qhr,kr->hqk/dot_general | solution.py:148
  133.3 1.0 convolution_convert_fusion
  134.4 3.2 %fusion.4 = f32[2,384,128]{2,1,0:T(8,128)S(1)} fusion(bf16[3072,2,128]{0,2,1:T(8,128)(2,1)S(1)} %bitcast.98, f32[2,384,3072]{1,2,0:T(8,128)S(1)} %get-tuple-element.41, f32[2,384]{1,0:T(2,128)S(1)} %broadcast_maximum_fusion, pred[384,3072]{0,1:T(8,128)(4,1)S(1)} %iota_compare_fusion), kind=kOutput, calls=%fused_computation.6 | convolution fusion | flops 611057664 | bytes 12585984 | tf_op jit(solution)/shard_map/cond/branch_1_fun/hqk,khd->hqd/dot_general | solution.py:158
  137.6 1.8 %fusion.3 = f32[2,384]{1,0:T(2,128)S(1)} fusion(f32[2,384,3072]{1,2,0:T(8,128)S(1)} %get-tuple-element.41, f32[2,384]{1,0:T(2,128)S(1)} %broadcast_maximum_fusion, pred[384,3072]{0,1:T(8,128)(4,1)S(1)} %iota_compare_fusion), kind=kLoop, calls=%fused_computation.5 | loop fusion | flops 7077120 | bytes 10622976 | tf_op jit(solution)/shard_map/cond/branch_1_fun/reduce_sum | solution.py:157
  140.0 9.2 %all_gather.20 = bf16[4,384,256]{2,1,0:T(8,128)(2,1)} all-gather(bf16[1,384,256]{2,1,0:T(8,128)(2,1)S(1)} %convert_element_type.89), channel_id=1, replica_groups=mesh['sp'=8,'tp'=4] {'tp'}, dimensions={0}, use_global_device_ids=true | all-gather | bytes 983040 | tf_op jit(solution)/shard_map/all_gather | solution.py:186
  149.2 2.1 %fusion.20 = f32[384,512]{1,0:T(8,128)S(1)} fusion(f32[384,512]{1,0:T(8,128)} %fusion.25, bf16[256,4,512]{2,0,1:T(8,128)(2,1)S(1)} %all-to-all-done.1, bf16[4,384,256]{2,1,0:T(8,128)(2,1)} %all_gather.20), kind=kOutput, calls=%fused_computation.35 | convolution fusion | flops 402849792 | bytes 3407872 | tf_op jit(solution)/shard_map/dot_general | solution.py:49
  151.3 1.3 fusion.26
  (79 shorter events, 1.8 us)
Async XLA Ops:
  6.5 38.8 %copy-start = (bf16[2048,512]{1,0:T(8,128)(2,1)S(1)}, bf16[2048,512]{1,0:T(8,128)(2,1)}, u32[]{:S(2)}) copy-start(bf16[2048,512]{1,0:T(8,128)(2,1)} %param.28) | copy-start | bytes 6291460
  6.5 36.4 %all-gather.3.cloned.1.call-start = ((), (), s32[]{:S(2)}) async-start(), calls=%async_computation.2 | async-start | bytes 1966080 | tf_op jit(solution)/shard_map/all_gather | solution.py:112
  9.5 4.4 %copy-start.22 = (f32[4]{0:T(128)S(1)}, f32[4]{0:T(128)}, u32[]{:S(2)}) copy-start(f32[4]{0:T(128)} %param.26) | copy-start | bytes 52
  9.5 26.5 %all-to-all-start = ((bf16[256,4,512]{0,2,1:T(8,128)(2,1)}), bf16[256,4,512]{0,2,1:T(8,128)(2,1)S(1)}, u32[]{:S(2)}, u32[]{:S(2)}) async-start(bf16[256,4,512]{0,2,1:T(8,128)(2,1)} %bitcast.100), calls=%async_computation | async-start | bytes 2097152 | tf_op jit(solution)/shard_map/all_to_all | solution.py:189
  36.1 1.0 copy-start.5
  37.0 112.1 %all-to-all-start.1 = ((bf16[256,4,512]{2,0,1:T(8,128)(2,1)}), bf16[256,4,512]{2,0,1:T(8,128)(2,1)S(1)}, u32[]{:S(2)}, u32[]{:S(2)}) async-start(bf16[256,4,512]{2,0,1:T(8,128)(2,1)} %copy.81), calls=%async_computation.1 | async-start | bytes 2097152 | tf_op jit(solution)/shard_map/all_to_all | solution.py:190
  40.6 84.8 %all-gather.5.cloned.1.call-start = ((), (), s32[]{:S(2)}) async-start(), calls=%async_computation.3 | async-start | bytes 3538944 | tf_op jit(solution)/shard_map/all_gather | solution.py:172
  40.6 4.2 %copy-start.17 = (f32[2048]{0:T(1024)S(1)}, f32[2048]{0:T(1024)}, u32[]{:S(2)}) copy-start(f32[2048]{0:T(1024)} %param.22) | copy-start | bytes 24580
  42.9 1.9 %copy-start.4 = (bf16[384,2048]{1,0:T(8,128)(2,1)S(1)}, bf16[384,2048]{1,0:T(8,128)(2,1)}, u32[]{:S(2)}) copy-start(bf16[384,2048]{1,0:T(8,128)(2,1)} %all-gather.3.cloned.1.call-done) | copy-start | bytes 4718596
  45.3 1.2 copy-start.2
  45.3 1.2 copy-start.19
  52.3 59.1 %collective-permute-start = (bf16[128,256]{0,1:T(8,128)(2,1)S(1)}, bf16[128,256]{0,1:T(8,128)(2,1)}, u32[]{:S(2)}, u32[]{:S(2)}) collective-permute-start(bf16[128,256]{0,1:T(8,128)(2,1)S(1)} %pad_maximum_fusion.4), channel_id=1, source_target_pairs={{0,4},{4,8},{8,12},{12,16},{16,20},{20,24},{24,28},{1,5},{5,9},{9,... | collective-permute-start | bytes 196616 | tf_op jit(solution)/shard_map/ppermute | solution.py:19
  64.1 38.0 %copy-start.3 = (bf16[384,2048]{1,0:T(8,128)(2,1)S(1)}, bf16[384,2048]{1,0:T(8,128)(2,1)}, u32[]{:S(2)}) copy-start(bf16[384,2048]{1,0:T(8,128)(2,1)} %copy-done.2) | copy-start | bytes 4718596
  102.1 2.7 %copy-start.15 = (bf16[512,128]{1,0:T(8,128)(2,1)S(1)}, bf16[512,128]{1,0:T(8,128)(2,1)}, u32[]{:S(2)}) copy-start(bf16[512,128]{1,0:T(8,128)(2,1)} %param.33) | copy-start | bytes 393220
  102.1 2.7 %copy-start.18 = (f32[512]{0:T(512)S(1)}, f32[512]{0:T(512)}, u32[]{:S(2)}) copy-start(f32[512]{0:T(512)} %param.30) | copy-start | bytes 6148
  104.8 1.0 copy-start.13
  104.8 2.0 %copy-start.20 = (bf16[2048,512]{1,0:T(8,128)(2,1)S(1)}, bf16[2048,512]{1,0:T(8,128)(2,1)}, u32[]{:S(2)}) copy-start(bf16[2048,512]{1,0:T(8,128)(2,1)} %param.39) | copy-start | bytes 6291460
  106.8 2.0 %copy-start.21 = (bf16[2048,512]{1,0:T(8,128)(2,1)S(1)}, bf16[2048,512]{1,0:T(8,128)(2,1)}, u32[]{:S(2)}) copy-start(bf16[2048,512]{1,0:T(8,128)(2,1)} %param.38) | copy-start | bytes 6291460
  112.3 2.4 %copy-start.12 = (pred[3,128,256]{1,2,0:T(8,128)(4,1)S(1)}, pred[3,128,256]{1,2,0:T(8,128)(4,1)}, u32[]{:S(2)}) copy-start(pred[3,128,256]{1,2,0:T(8,128)(4,1)} %broadcast_and_fusion) | copy-start | bytes 294916
  113.0 2.1 %copy-start.16 = (bf16[3,128,2,64]{1,3,2,0:T(8,128)(2,1)S(1)}, bf16[3,128,2,64]{1,3,2,0:T(8,128)(2,1)}, u32[]{:S(2)}) copy-start(bf16[3,128,2,64]{1,3,2,0:T(8,128)(2,1)} %copy.70) | copy-start | bytes 294916
  126.3 3.0 %copy-start.10 = (bf16[384,256]{1,0:T(8,128)(2,1)S(1)}, bf16[384,256]{1,0:T(8,128)(2,1)}, u32[]{:S(2)}) copy-start(bf16[384,256]{1,0:T(8,128)(2,1)} %get-tuple-element.28) | copy-start | bytes 589828 | tf_op jit(solution)/shard_map/cond
  129.3 1.6 %copy-start.8 = (bf16[3072,64]{0,1:T(8,128)(2,1)S(1)}, bf16[3072,64]{0,1:T(8,128)(2,1)}, u32[]{:S(2)}) copy-start(bf16[3072,64]{0,1:T(8,128)(2,1)} %get-tuple-element.29) | copy-start | bytes 1179652 | tf_op jit(solution)/shard_map/cond
  129.3 1.6 %copy-start.11 = (bf16[384,2,64]{0,2,1:T(8,128)(2,1)S(1)}, bf16[384,2,64]{0,2,1:T(8,128)(2,1)}, u32[]{:S(2)}) copy-start(bf16[384,2,64]{0,2,1:T(8,128)(2,1)} %get-tuple-element.30) | copy-start | bytes 294916 | tf_op jit(solution)/shard_map/cond
  130.9 2.4 %copy-start.1 = (bf16[3072,512]{1,0:T(8,128)(2,1)S(1)}, bf16[3072,512]{1,0:T(8,128)(2,1)}, u32[]{:S(2)}) copy-start(bf16[3072,512]{1,0:T(8,128)(2,1)} %get-tuple-element.26) | copy-start | bytes 9437188 | tf_op jit(solution)/shard_map/cond
  130.9 2.4 %copy-start.14 = (bf16[512,256]{1,0:T(8,128)(2,1)S(1)}, bf16[512,256]{1,0:T(8,128)(2,1)}, u32[]{:S(2)}) copy-start(bf16[512,256]{1,0:T(8,128)(2,1)} %get-tuple-element.39) | copy-start | bytes 786436 | tf_op jit(solution)/shard_map/cond
  149.2 2.1 %copy-start.6 = (bf16[4,256,512]{2,1,0:T(8,128)(2,1)S(1)}, bf16[4,256,512]{2,1,0:T(8,128)(2,1)}, u32[]{:S(2)}) copy-start(bf16[4,256,512]{2,1,0:T(8,128)(2,1)} %copy.78) | copy-start | bytes 3145732
  149.2 2.1 %copy-start.7 = (bf16[384,1024]{0,1:T(8,128)(2,1)S(1)}, bf16[384,1024]{0,1:T(8,128)(2,1)}, u32[]{:S(2)}) copy-start(bf16[384,1024]{0,1:T(8,128)(2,1)} %all_gather.17) | copy-start | bytes 2359300
  149.2 2.2 %copy-start.9 = (f32[384,512]{1,0:T(8,128)S(1)}, f32[384,512]{1,0:T(8,128)}, u32[]{:S(2)}) copy-start(f32[384,512]{1,0:T(8,128)} %fusion.23) | copy-start | bytes 2359300
Sparse Core Ops, SparseCore 0:
  8.9 29.3 all-gather.2
  47.5 67.1 all-gather.4
